TPU v7x, 32 devices: a whole 2x2x4 slice. The times are simulated.
32 devices in a mesh: fs: 8 (over z, y), tp: 4 (over x, core).
Axes of the slice: x: 2, y: 2, z: 4, core: 2. Of those that a mesh axis runs over, the one named last changes fastest.
Arguments:
- cotangent: bfloat16 [5120, 1024], P('fs', 'tp'), may hold values from -6 to 6
- inputs: bfloat16 [5120, 1024], P('fs', 'tp'), may hold values from -6 to 6
- pre_act: bfloat16 [5120, 2112], P('fs'), may hold values from -6 to 6
- w_up: bfloat16 [2112, 1024], P('fs', 'tp'), may hold values from -0.1875 to 0.1875
- w_down: bfloat16 [2112, 1024], P('fs', 'tp'), may hold values from -0.125 to 0.125
Outputs:
- grad_input: bfloat16 [5120, 1024], P('fs', 'tp')
- grad_up: float32 [2112, 1024], P('fs', 'tp')
All inputs are finite; a program needn't handle non-finite values.
Results may differ from a plain program's by a relative error of at most 0.0049.
Values may be sent and summed in bfloat16 or wider, within the bound.
A program may use at most 64 MiB of HBM per device.

v0:
```python
import jax
import jax.numpy as jnp
from jax import lax
from jax.sharding import PartitionSpec as P


def times_rows(left, piece):
    return lax.dot_general(
        left, piece, (((1,), (1,)), ((), ())), preferred_element_type=jnp.float32
    )


def local(cotangent, inputs, pre_act, w_up, w_down):
    row_count = cotangent.shape[0]
    token_total = row_count * lax.axis_size("fs")
    full_cotangent = lax.all_gather(cotangent, "tp", axis=1, tiled=True)
    down_whole = lax.all_gather(w_down, "tp", axis=1, tiled=True)
    grad_hidden = times_rows(full_cotangent, lax.all_gather(down_whole, "fs", axis=0, tiled=True))
    grad_pre = (2.0 * grad_hidden * jnp.maximum(pre_act.astype(jnp.float32), 0.0)).astype(
        jnp.bfloat16
    )
    columns = grad_pre
    grad_input = jnp.dot(
        columns, lax.all_gather(w_up, "fs", axis=0, tiled=True), preferred_element_type=jnp.float32
    )
    columns = grad_pre
    grad_share = lax.psum_scatter(
        lax.dot_general(
            columns, inputs, (((0,), (0,)), ((), ())), preferred_element_type=jnp.float32
        ),
        "fs",
        scatter_dimension=0,
        tiled=True,
    )
    grad_up = grad_share / jnp.sqrt(jnp.float32(token_total))
    return (grad_input.astype(jnp.bfloat16), grad_up)


def solution(mesh):
    return jax.shard_map(
        local,
        mesh=mesh,
        in_specs=(P("fs", "tp"), P("fs", "tp"), P("fs", None), P("fs", "tp"), P("fs", "tp")),
        out_specs=(P("fs", "tp"), P("fs", "tp")),
        check_vma=False,
    )
```

profile of v0, /device:TPU:0, one launch (start us, length us, event | category | flops | bytes accessed | tf_op | source)
XLA Modules:
  0.0 227.8 jit_solution(900045571831877215)
XLA Ops:
  7.2 0.0 copy-start
  7.2 0.0 all-gather.4.cloned.1.call-start
  7.2 0.7 all-gather.4.cloned.1.call-update
  7.9 0.0 all-gather.6.cloned.1.call-start
  8.0 10.3 %all_gather.13 = bf16[264,1024]{1,0:T(8,128)(2,1)} all-gather(bf16[264,256]{1,0:T(8,128)(2,1)} %param.9), channel_id=1, replica_groups=mesh['fs'=8,'tp'=4] {'tp'}, dimensions={1}, use_global_device_ids=true | all-gather | bytes 675840 | tf_op jit(solution)/shard_map/all_gather | solution.py:17
  18.3 0.0 all-gather.6.cloned.1.call-update
  18.3 0.0 all-gather.8.cloned.1.call-start
  18.4 0.7 all-gather.8.cloned.1.call-update
  19.1 0.0 reduce-scatter.2.cloned.1.call-start
  19.1 11.5 %all-gather.4.cloned.1.call-done = bf16[640,1024]{1,0:T(8,128)(2,1)} async-done(((bf16[640,256]{1,0:T(8,128)(2,1)}), bf16[640,1024]{1,0:T(8,128)(2,1)}) %all-gather.4.cloned.1.call-update) | async-done | bytes 1310736 | tf_op jit(solution)/shard_map/all_gather | solution.py:16
  30.6 76.6 %all-gather.6.cloned.1.call-done = bf16[2112,1024]{1,0:T(8,128)(2,1)} async-done(((bf16[264,1024]{1,0:T(8,128)(2,1)}), bf16[2112,1024]{1,0:T(8,128)(2,1)}) %all-gather.6.cloned.1.call-update) | async-done | bytes 4325392 | tf_op jit(solution)/shard_map/all_gather | solution.py:18
  107.2 7.1 %fusion.1 = bf16[640,2112]{0,1:T(8,128)(2,1)S(1)} fusion(bf16[640,2112]{0,1:T(8,128)(2,1)} %param.7, bf16[640,1024]{1,0:T(8,128)(2,1)} %all-gather.4.cloned.1.call-done, bf16[2112,1024]{1,0:T(8,128)(2,1)} %all-gather.6.cloned.1.call-done), kind=kOutput, calls=%fused_computation.2 | convolution fusion | flops 2774999040 | bytes 11042816 | tf_op jit(solution)/shard_map/dot_general | solution.py:8
  114.4 0.0 copy-done
  114.4 2.4 %fusion.2 = f32[2112,256]{1,0:T(8,128)} fusion(bf16[640,2112]{0,1:T(8,128)(2,1)S(1)} %fusion.1, bf16[640,256]{1,0:T(8,128)(2,1)S(1)} %copy-done), kind=kOutput, calls=%fused_computation.5 | convolution fusion | flops 692060160 | bytes 5193728 | tf_op jit(solution)/shard_map/dot_general | solution.py:28
  116.7 0.0 reduce-scatter.2.cloned.1.call-update
  116.8 31.7 %all-gather.8.cloned.1.call-done = bf16[2112,256]{1,0:T(8,128)(2,1)} async-done(((bf16[264,256]{1,0:T(8,128)(2,1)}), bf16[2112,256]{1,0:T(8,128)(2,1)}) %all-gather.8.cloned.1.call-update) | async-done | bytes 1081360 | tf_op jit(solution)/shard_map/all_gather | solution.py:24
  148.5 2.9 %convolution_convert_fusion = bf16[640,256]{1,0:T(8,128)(2,1)} fusion(bf16[640,2112]{0,1:T(8,128)(2,1)S(1)} %fusion.1, bf16[2112,256]{1,0:T(8,128)(2,1)} %all-gather.8.cloned.1.call-done), kind=kOutput, calls=%fused_computation.3 | convolution fusion | flops 692224000 | bytes 4112384 | tf_op jit(solution)/shard_map/dot_general | solution.py:23
  151.4 68.2 %reduce-scatter.2.cloned.1.call-done = f32[264,256]{1,0:T(8,128)} async-done(((f32[2112,256]{1,0:T(8,128)}), f32[264,256]{1,0:T(8,128)}) %reduce-scatter.2.cloned.1.call-update) | async-done | bytes 270352 | tf_op jit(solution)/shard_map/reduce_scatter | solution.py:27
  219.6 1.7 broadcast_multiply_fusion
Async XLA Ops:
  7.2 107.2 %copy-start = (bf16[640,256]{1,0:T(8,128)(2,1)S(1)}, bf16[640,256]{1,0:T(8,128)(2,1)}, u32[]{:S(2)}) copy-start(bf16[640,256]{1,0:T(8,128)(2,1)} %param.6) | copy-start | bytes 983044
  7.2 23.4 %all-gather.4.cloned.1.call-start = ((), (), s32[]{:S(2)}) async-start(), calls=%async_computation.1 | async-start | bytes 1638400 | tf_op jit(solution)/shard_map/all_gather | solution.py:16
  7.9 99.3 %all-gather.6.cloned.1.call-start = ((), (), s32[]{:S(2)}) async-start(), calls=%async_computation.2 | async-start | bytes 4866048 | tf_op jit(solution)/shard_map/all_gather | solution.py:18
  18.3 130.1 %all-gather.8.cloned.1.call-start = ((), (), s32[]{:S(2)}) async-start(), calls=%async_computation.3 | async-start | bytes 1216512 | tf_op jit(solution)/shard_map/all_gather | solution.py:24
  19.1 200.5 %reduce-scatter.2.cloned.1.call-start = ((), (), s32[]{:S(2)}) async-start(), calls=%async_computation.4 | async-start | bytes 2433024 | tf_op jit(solution)/shard_map/reduce_scatter | solution.py:27
Sparse Core Ops, SparseCore 0:
  9.5 21.0 all-gather.3
  32.8 74.3 all-gather.5
  109.4 39.0 all-gather.7
  151.8 67.7 reduce-scatter.1
where the time goes:
time: 228 us
  waiting for transfers between devices  189 us (83%)
  between operations  13.8 us (6%)
  matrix products  12.4 us (5%)
  blocking collectives  10.3 us (5%)
    all_gather x1, waiting for transfers between devices, local(): lax.all_gather(down_whole, 'fs', axis=0, tiled=True)  76.6 us
    reduce_scatter x1, waiting for transfers between devices, local(): lax.psum_scatter(lax.dot_general(columns, inputs, (((0,), (0,)), ((), ())...  68.2 us
    all_gather x1, waiting for transfers between devices, local(): lax.all_gather(w_up, 'fs', axis=0, tiled=True)  31.7 us
    all_gather x1, waiting for transfers between devices, local(): full_cotangent = lax.all_gather(cotangent, 'tp', axis=1, tiled=True)  11.5 us
    all_gather x1, blocking collectives, local(): down_whole = lax.all_gather(w_down, 'tp', axis=1, tiled=True)  10.3 us
    dot_general x1, matrix products, times_rows(): lax.dot_general(left, piece, (((1,), (1,)), ((), ())), preferred_element_...  7.12 us
  transfers between devices with their start and end apart: 4, of which 4 were waited for; matrix products, arithmetic and copies ran while one was open for 5% of the time, Pallas kernels for 0%

commit v1 on v0

--- a/solution.py
+++ b/solution.py
@@ -13,7 +13,12 @@
 def local(cotangent, inputs, pre_act, w_up, w_down):
     row_count = cotangent.shape[0]
     token_total = row_count * lax.axis_size("fs")
-    full_cotangent = lax.all_gather(cotangent, "tp", axis=1, tiled=True)
+    ring = [cotangent]
+    for hop in range(3):
+        ring.append(lax.ppermute(ring[-1], "tp", [(dev, (dev + 1) % 4) for dev in range(4)]))
+    full_cotangent = jnp.roll(
+        jnp.concatenate(ring[::-1], axis=1), (lax.axis_index("tp") + 1) * ring[0].shape[1], axis=1
+    )
     down_whole = lax.all_gather(w_down, "tp", axis=1, tiled=True)
     grad_hidden = times_rows(full_cotangent, lax.all_gather(down_whole, "fs", axis=0, tiled=True))
     grad_pre = (2.0 * grad_hidden * jnp.maximum(pre_act.astype(jnp.float32), 0.0)).astype(

time: 228 us -> 213 us (0.934)
  waiting for transfers between devices: 189 us -> 168 us
  local copies, waits for them, and re-layouts: 0.01 us -> 6.31 us
    all_gather x1, waiting for transfers between devices: 76.6 us -> 48.8 us  [local(): lax.all_gather(down_whole, 'fs', axis=0, tiled=True)]
    ppermute x0 -> x3, waiting for transfers between devices: none -> 19.3 us  [local(): lax.ppermute(ring[-1], 'tp', [(dev, (dev + 1) % 4) for dev in range(4)])]
    all_gather x1 -> x0, waiting for transfers between devices: 11.5 us -> none  [local(): full_cotangent = lax.all_gather(cotangent, 'tp', axis=1, tiled=True)]
    unnamed x2 -> x11, local copies, waits for them, and re-layouts: 0.01 us -> 5.52 us
  transfers between devices with their start and end apart: 4 -> 6, of which waited for: 4 -> 6; matrix products, arithmetic and copies ran while one was open for 5% -> 9% of each run, Pallas kernels for 0% -> 0%
where the time goes in v1:
time: 213 us
  waiting for transfers between devices  168 us (79%)
  between operations  13.8 us (6%)
  matrix products  12.4 us (6%)
  blocking collectives  10.5 us (5%)
  local copies, waits for them, and re-layouts  6.31 us (3%)
    reduce_scatter x1, waiting for transfers between devices, local(): lax.psum_scatter(lax.dot_general(columns, inputs, (((0,), (0,)), ((), ())...  68.3 us
    all_gather x1, waiting for transfers between devices, local(): lax.all_gather(down_whole, 'fs', axis=0, tiled=True)  48.8 us
    all_gather x1, waiting for transfers between devices, local(): lax.all_gather(w_up, 'fs', axis=0, tiled=True)  31.7 us
    ppermute x3, waiting for transfers between devices, local(): lax.ppermute(ring[-1], 'tp', [(dev, (dev + 1) % 4) for dev in range(4)])  19.3 us
    all_gather x1, blocking collectives, local(): down_whole = lax.all_gather(w_down, 'tp', axis=1, tiled=True)  10.5 us
    dot_general x1, matrix products, times_rows(): lax.dot_general(left, piece, (((1,), (1,)), ((), ())), preferred_element_...  7.12 us
    unnamed x11, local copies, waits for them, and re-layouts  5.52 us
  transfers between devices with their start and end apart: 6, of which 6 were waited for; matrix products, arithmetic and copies ran while one was open for 9% of the time, Pallas kernels for 0%

profile of v1, /device:TPU:0, one launch (start us, length us, event | category | flops | bytes accessed | tf_op | source)
XLA Modules:
  0.0 213.3 jit_solution(4555875753944493104)
XLA Ops:
  7.2 0.0 copy-start
  7.2 0.0 copy-start.1
  7.2 0.0 all-gather.3.cloned.1.call-start
  7.2 10.5 %all_gather.9 = bf16[264,1024]{1,0:T(8,128)(2,1)} all-gather(bf16[264,256]{1,0:T(8,128)(2,1)} %param.9), channel_id=1, replica_groups=mesh['fs'=8,'tp'=4] {'tp'}, dimensions={1}, use_global_device_ids=true | all-gather | bytes 675840 | tf_op jit(solution)/shard_map/all_gather | solution.py:22
  17.7 0.0 all-gather.3.cloned.1.call-update
  17.7 0.0 all-gather.5.cloned.1.call-start
  17.8 0.4 collective-permute-start
  18.2 6.4 %collective-permute-done = bf16[640,256]{1,0:T(8,128)(2,1)S(1)} collective-permute-done((bf16[640,256]{1,0:T(8,128)(2,1)}, bf16[640,256]{1,0:T(8,128)(2,1)S(1)}, u32[]{:S(2)}, u32[]{:S(2)}) %collective-permute-start) | collective-permute-done | bytes 327712 | tf_op jit(solution)/shard_map/ppermute | solution.py:18
  24.5 0.0 collective-permute-start.1
  24.5 6.5 %collective-permute-done.1 = bf16[640,256]{1,0:T(8,128)(2,1)S(1)} collective-permute-done((bf16[640,256]{1,0:T(8,128)(2,1)S(1)}, bf16[640,256]{1,0:T(8,128)(2,1)S(1)}, u32[]{:S(2)}, u32[]{:S(2)}) %collective-permute-start.1) | collective-permute-done | bytes 327712 | tf_op jit(solution)/shard_map/ppermute | solution.py:18
  31.0 0.0 collective-permute-start.2
  31.0 0.0 all-gather.5.cloned.1.call-update
  31.1 0.0 reduce-scatter.2.cloned.1.call-start
  31.1 6.4 %collective-permute-done.2 = bf16[640,256]{1,0:T(8,128)(2,1)S(1)} collective-permute-done((bf16[640,256]{1,0:T(8,128)(2,1)S(1)}, bf16[640,256]{1,0:T(8,128)(2,1)S(1)}, u32[]{:S(2)}, u32[]{:S(2)}) %collective-permute-start.2) | collective-permute-done | bytes 327712 | tf_op jit(solution)/shard_map/ppermute | solution.py:18
  37.5 0.8 constant_dynamic-update-slice_fusion.7
  38.3 0.8 constant_dynamic-update-slice_fusion.6
  39.1 0.8 constant_dynamic-update-slice_fusion.5
  39.9 0.0 copy-done.1
  39.9 0.8 constant_dynamic-update-slice_fusion.4
  40.7 0.8 constant_dynamic-update-slice_fusion.3
  41.5 0.8 constant_dynamic-update-slice_fusion.2
  42.3 0.8 constant_dynamic-update-slice_fusion.1
  43.1 0.8 constant_dynamic-update-slice_fusion
  43.8 48.8 %all-gather.3.cloned.1.call-done = bf16[2112,1024]{1,0:T(8,128)(2,1)} async-done(((bf16[264,1024]{1,0:T(8,128)(2,1)}), bf16[2112,1024]{1,0:T(8,128)(2,1)}) %all-gather.3.cloned.1.call-update) | async-done | bytes 4325392 | tf_op jit(solution)/shard_map/all_gather | solution.py:23
  92.6 7.1 %fusion.1 = bf16[640,2112]{0,1:T(8,128)(2,1)S(1)} fusion(bf16[640,2112]{0,1:T(8,128)(2,1)} %param.7, bf16[2112,1024]{1,0:T(8,128)(2,1)} %all-gather.3.cloned.1.call-done, bf16[640,2048]{1,0:T(8,128)(2,1)} %constant_dynamic-update-slice_fusion, s32[]{:T(128)S(6)} %select_n.14), kind=kOutput, calls=%fused_computation.2 | convolution fusion | flops 2774999040 | bytes 11042820 | tf_op jit(solution)/shard_map/dot_general | solution.py:8
  99.7 0.0 copy-done
  99.8 2.4 %fusion.4 = f32[2112,256]{1,0:T(8,128)} fusion(bf16[640,2112]{0,1:T(8,128)(2,1)S(1)} %fusion.1, bf16[640,256]{1,0:T(8,128)(2,1)S(1)} %copy-done), kind=kOutput, calls=%fused_computation.15 | convolution fusion | flops 692060160 | bytes 5193728 | tf_op jit(solution)/shard_map/dot_general | solution.py:33
  102.1 0.0 reduce-scatter.2.cloned.1.call-update
  102.1 31.7 %all-gather.5.cloned.1.call-done = bf16[2112,256]{1,0:T(8,128)(2,1)} async-done(((bf16[264,256]{1,0:T(8,128)(2,1)}), bf16[2112,256]{1,0:T(8,128)(2,1)}) %all-gather.5.cloned.1.call-update) | async-done | bytes 1081360 | tf_op jit(solution)/shard_map/all_gather | solution.py:29
  133.8 2.9 %convolution_convert_fusion = bf16[640,256]{1,0:T(8,128)(2,1)} fusion(bf16[640,2112]{0,1:T(8,128)(2,1)S(1)} %fusion.1, bf16[2112,256]{1,0:T(8,128)(2,1)} %all-gather.5.cloned.1.call-done), kind=kOutput, calls=%fused_computation.4 | convolution fusion | flops 692224000 | bytes 4112384 | tf_op jit(solution)/shard_map/dot_general | solution.py:28
  136.8 68.3 %reduce-scatter.2.cloned.1.call-done = f32[264,256]{1,0:T(8,128)} async-done(((f32[2112,256]{1,0:T(8,128)}), f32[264,256]{1,0:T(8,128)}) %reduce-scatter.2.cloned.1.call-update) | async-done | bytes 270352 | tf_op jit(solution)/shard_map/reduce_scatter | solution.py:32
  205.0 1.7 broadcast_multiply_fusion
Async XLA Ops:
  7.2 92.6 %copy-start = (bf16[640,256]{1,0:T(8,128)(2,1)S(1)}, bf16[640,256]{1,0:T(8,128)(2,1)}, u32[]{:S(2)}) copy-start(bf16[640,256]{1,0:T(8,128)(2,1)} %param.6) | copy-start | bytes 983044
  7.2 32.7 %copy-start.1 = (bf16[640,256]{1,0:T(8,128)(2,1)S(1)}, bf16[640,256]{1,0:T(8,128)(2,1)}, u32[]{:S(2)}) copy-start(bf16[640,256]{1,0:T(8,128)(2,1)} %param.5) | copy-start | bytes 983044
  7.2 85.4 %all-gather.3.cloned.1.call-start = ((), (), s32[]{:S(2)}) async-start(), calls=%async_computation.1 | async-start | bytes 4866048 | tf_op jit(solution)/shard_map/all_gather | solution.py:23
  17.7 116.1 %all-gather.5.cloned.1.call-start = ((), (), s32[]{:S(2)}) async-start(), calls=%async_computation.2 | async-start | bytes 1216512 | tf_op jit(solution)/shard_map/all_gather | solution.py:29
  17.8 6.8 %collective-permute-start = (bf16[640,256]{1,0:T(8,128)(2,1)}, bf16[640,256]{1,0:T(8,128)(2,1)S(1)}, u32[]{:S(2)}, u32[]{:S(2)}) collective-permute-start(bf16[640,256]{1,0:T(8,128)(2,1)} %param.5), channel_id=1, source_target_pairs={{0,1},{1,2},{2,3},{3,0},{4,5},{5,6},{6,7},{7,4},{8,9},{9,10},{10,1... | collective-permute-start | bytes 983048 | tf_op jit(solution)/shard_map/ppermute | solution.py:18
  24.5 6.5 %collective-permute-start.1 = (bf16[640,256]{1,0:T(8,128)(2,1)S(1)}, bf16[640,256]{1,0:T(8,128)(2,1)S(1)}, u32[]{:S(2)}, u32[]{:S(2)}) collective-permute-start(bf16[640,256]{1,0:T(8,128)(2,1)S(1)} %collective-permute-done), channel_id=1, source_target_pairs={{0,1},{1,2},{2,3},{3,0},{4,5},{5,6},{6,7},{7,4},{8,9},{9,10},{10,1... | collective-permute-start | bytes 983048 | tf_op jit(solution)/shard_map/ppermute | solution.py:18
  31.0 6.5 %collective-permute-start.2 = (bf16[640,256]{1,0:T(8,128)(2,1)S(1)}, bf16[640,256]{1,0:T(8,128)(2,1)S(1)}, u32[]{:S(2)}, u32[]{:S(2)}) collective-permute-start(bf16[640,256]{1,0:T(8,128)(2,1)S(1)} %collective-permute-done.1), channel_id=1, source_target_pairs={{0,1},{1,2},{2,3},{3,0},{4,5},{5,6},{6,7},{7,4},{8,9},{9,10},{10,1... | collective-permute-start | bytes 983048 | tf_op jit(solution)/shard_map/ppermute | solution.py:18
  31.1 174.0 %reduce-scatter.2.cloned.1.call-start = ((), (), s32[]{:S(2)}) async-start(), calls=%async_computation.3 | async-start | bytes 2433024 | tf_op jit(solution)/shard_map/reduce_scatter | solution.py:32
Sparse Core Ops, SparseCore 0:
  17.8 74.7 all-gather.2
  94.8 39.0 all-gather.4
  137.3 67.6 reduce-scatter.1
